TPU v7x, 32 devices: a whole 2x2x4 slice. The times are simulated.
32 devices in a mesh: sp: 8 (over z, y), dp: 4 (over x, core).
Axes of the slice: x: 2, y: 2, z: 4, core: 2. Of those that a mesh axis runs over, the one named last changes fastest.
Arguments:
- hidden_in: bfloat16 [4, 1024, 2048], P('dp', 'sp'), may hold values from -6 to 6
- queries: bfloat16 [4, 1024, 1536], P('dp', 'sp'), may hold values from -64 to 64
- key_value_latent: bfloat16 [4, 1024, 512], P('dp', 'sp'), may hold values from -6 to 6
- keys_rope: bfloat16 [4, 1024, 32], P('dp', 'sp'), may hold values from -4 to 4
- latent_norm_gain: float32 [512], replicated, may hold values from 0.1 to 1.9
- latent_up_weight: bfloat16 [512, 2048], replicated, may hold values from -0.25 to 0.25
- attn_gain: float32 [1024], replicated, may hold values from 0.1 to 1.9
- out_proj: bfloat16 [1024, 2048], replicated, may hold values from -0.1875 to 0.1875
- norm1_gain: float32 [2048], replicated, may hold values from 0.1 to 1.9
- norm1_bias: float32 [2048], replicated, may hold values from -1.5 to 1.5
- expert_ids: int32 [4, 1024, 4], P('dp', 'sp'), may hold values from 0 to 31, all different within a row; in each aligned block of 128 rows (0 to 127, 128 to 255, ..., all dimensions but the last counted through in order) at most 24 rows name the same one
- route_weights: float32 [4, 1024, 4], P('dp', 'sp'), may hold values from 0.1 to 1
- gate_proj: bfloat16 [32, 2048, 512], P(('sp', 'dp')), may hold values from -0.125 to 0.125
- up_proj: bfloat16 [32, 2048, 512], P(('sp', 'dp')), may hold values from -0.125 to 0.125
- down_proj: bfloat16 [32, 512, 2048], P(('sp', 'dp')), may hold values from -0.25 to 0.25
- shared_gate: bfloat16 [2048, 512], replicated, may hold values from -0.125 to 0.125
- shared_up: bfloat16 [2048, 512], replicated, may hold values from -0.125 to 0.125
- shared_down: bfloat16 [512, 2048], replicated, may hold values from -0.25 to 0.25
- norm2_gain: float32 [2048], replicated, may hold values from 0.1 to 1.9
- norm2_bias: float32 [2048], replicated, may hold values from -1.5 to 1.5
Outputs:
- result: bfloat16 [4, 1024, 2048], P('dp', 'sp')
Inputs may be any that keep to these rules, and one draw needn't show every extreme that they name: `expert_ids`: each row names 4 different experts. Among the rows of one device (aligned blocks of 128 rows), no expert is named more than 24 times, a bound that some block reaches.
All inputs are finite; a program needn't handle non-finite values.
Results may differ from a plain program's by a relative error of at most 0.01.
Values may be sent and summed in bfloat16 or wider, within the bound.
A program may use at most 128 MiB of HBM per device.

v0:
```python
import math

import jax
import jax.numpy as jnp
from jax import lax
from jax.sharding import PartitionSpec as P

D = 2048
ATTENTION_HEADS = 16
PLAIN_HEAD_WIDTH = 64
QK_ROPE = 32
VALUE_HEAD_WIDTH = 64
TOP_K = 4


ALPHA = 2.0**0.25
ROUTED = 2.5
THETA = 10000.0


def rms_scaled(values, scaling):
    widened = values.astype(jnp.float32)
    return (
        widened * lax.rsqrt(jnp.mean(widened * widened, axis=-1, keepdims=True) + 1e-06) * scaling
    )


def layer_norm(values, scaling, bias_add):
    centre = values - jnp.mean(values, axis=-1, keepdims=True)
    spread = jnp.mean(centre * centre, axis=-1, keepdims=True)
    return centre * lax.rsqrt(spread + 1e-05) * scaling + bias_add


def rotation_tables(positions, rot_width):
    frequency = THETA ** (-jnp.arange(0, rot_width, 2, dtype=jnp.float32) / rot_width)
    angles = positions.astype(jnp.float32)[:, None] * frequency[None, :]
    return (jnp.cos(angles), jnp.sin(angles))


def turn(values, cosine_table, sine_table):
    half_width = values.shape[-1] // 2
    first_half = values[..., :half_width]
    second_half = values[..., half_width:]
    return jnp.concatenate(
        [
            first_half * cosine_table - second_half * sine_table,
            second_half * cosine_table + first_half * sine_table,
        ],
        axis=-1,
    )


def attend(query, key_full, values):
    length = query.shape[0]
    span_rows = 512
    block_count = length // span_rows
    blocks = query.reshape(block_count, span_rows, query.shape[1])
    key_pos = jnp.arange(length, dtype=jnp.int32)
    factor = 1.0 / math.sqrt(query.shape[1])

    def one_block(inputs):
        block_index, query_rows = inputs
        scores = jnp.dot(query_rows, key_full.T, preferred_element_type=jnp.float32) * factor
        query_pos = block_index * span_rows + jnp.arange(span_rows, dtype=jnp.int32)
        scores = jnp.where(key_pos[None, :] <= query_pos[:, None], scores, -jnp.inf)
        row_max = jnp.max(scores, axis=-1, keepdims=True)
        weights = jnp.exp(scores - row_max)
        weights = (weights / jnp.sum(weights, axis=-1, keepdims=True)).astype(jnp.bfloat16)
        return jnp.dot(weights, values, preferred_element_type=jnp.float32).astype(jnp.bfloat16)

    attended = lax.map(one_block, (jnp.arange(block_count, dtype=jnp.int32), blocks))
    return attended.reshape(length, values.shape[1])


def swiglu_rows(rows, gate_mat, up_mat, down_mat):
    gated = jnp.dot(rows, gate_mat, preferred_element_type=jnp.float32)
    lifted = jnp.dot(rows, up_mat, preferred_element_type=jnp.float32)
    inner = (jax.nn.silu(gated) * lifted).astype(jnp.bfloat16)
    return jnp.dot(inner, down_mat, preferred_element_type=jnp.float32)


def per_device(
    hidden_in,
    queries,
    key_value_latent,
    keys_rope,
    latent_norm_gain,
    latent_up_weight,
    attn_gain,
    out_proj,
    norm1_gain,
    norm1_bias,
    expert_ids,
    route_weights,
    gate_proj,
    up_proj,
    down_proj,
    shared_gate,
    shared_up,
    shared_down,
    norm2_gain,
    norm2_bias,
):
    seq_devices = lax.axis_size("sp")
    tok_rows = hidden_in.shape[1]
    length = tok_rows * seq_devices
    heads_here = ATTENTION_HEADS // seq_devices
    normed = rms_scaled(key_value_latent[0], latent_norm_gain).astype(jnp.bfloat16)
    keys_values = jnp.dot(normed, latent_up_weight, preferred_element_type=jnp.float32).astype(
        jnp.bfloat16
    )
    local_pos = lax.axis_index("sp") * tok_rows + jnp.arange(tok_rows, dtype=jnp.int32)
    cos_local, sin_local = rotation_tables(local_pos, QK_ROPE)
    keys_turned = turn(keys_rope[0].astype(jnp.float32), cos_local, sin_local).astype(jnp.bfloat16)
    query_send = queries[0].reshape(
        tok_rows, seq_devices, heads_here * (PLAIN_HEAD_WIDTH + QK_ROPE)
    )
    pair_send = keys_values.reshape(
        tok_rows, seq_devices, heads_here * (PLAIN_HEAD_WIDTH + VALUE_HEAD_WIDTH)
    )
    query_heads, pair_heads = (
        lax.all_to_all(query_send, "sp", split_axis=1, concat_axis=0, tiled=True),
        lax.all_to_all(pair_send, "sp", split_axis=1, concat_axis=0, tiled=True),
    )
    keys_whole = lax.all_gather(keys_turned, "sp", axis=0, tiled=True)
    query_heads = query_heads.reshape(length, heads_here, PLAIN_HEAD_WIDTH + QK_ROPE)
    pair_heads = pair_heads.reshape(length, heads_here, PLAIN_HEAD_WIDTH + VALUE_HEAD_WIDTH)
    cos_whole, sin_whole = rotation_tables(jnp.arange(length, dtype=jnp.int32), QK_ROPE)
    query_turned = turn(
        query_heads[..., PLAIN_HEAD_WIDTH:].astype(jnp.float32),
        cos_whole[:, None, :],
        sin_whole[:, None, :],
    ).astype(jnp.bfloat16)
    query_full = jnp.concatenate([query_heads[..., :PLAIN_HEAD_WIDTH], query_turned], axis=-1)
    key_full = jnp.concatenate(
        [
            pair_heads[..., :PLAIN_HEAD_WIDTH],
            jnp.broadcast_to(keys_whole[:, None, :], (length, heads_here, QK_ROPE)),
        ],
        axis=-1,
    )
    values_heads = pair_heads[..., PLAIN_HEAD_WIDTH:]
    by_head = lax.map(
        lambda inputs: attend(inputs[0], inputs[1], inputs[2]),
        (
            jnp.moveaxis(query_full, 1, 0),
            jnp.moveaxis(key_full, 1, 0),
            jnp.moveaxis(values_heads, 1, 0),
        ),
    )
    outgoing = jnp.moveaxis(by_head, 0, 1).reshape(
        seq_devices, tok_rows, heads_here * VALUE_HEAD_WIDTH
    )
    incoming = lax.all_to_all(outgoing, "sp", split_axis=0, concat_axis=2, tiled=True)
    attn_normed = rms_scaled(incoming[0], attn_gain).astype(jnp.bfloat16)
    mixed = jnp.dot(attn_normed, out_proj, preferred_element_type=jnp.float32)
    first = layer_norm(
        ALPHA * hidden_in[0].astype(jnp.float32) + mixed, norm1_gain, norm1_bias
    ).astype(jnp.bfloat16)
    group = lax.axis_size("sp") * lax.axis_size("dp")
    capacity = (tok_rows * TOP_K * 3 + 2 * group - 1) // (2 * group)
    entries = expert_ids[0].reshape(-1)
    onehot = (entries[:, None] == jnp.arange(group, dtype=jnp.int32)[None, :]).astype(jnp.int32)
    earlier = jnp.cumsum(onehot, axis=0) - onehot
    slots = jnp.sum(earlier * onehot, axis=-1)
    places = (entries * capacity + slots).reshape(tok_rows, TOP_K)
    slot_ids = jnp.arange(group * capacity, dtype=jnp.int32)
    dispatch = jnp.any(places[None, :, :] == slot_ids[:, None, None], axis=-1).astype(jnp.bfloat16)
    outbound = jnp.dot(dispatch, first, preferred_element_type=jnp.float32).astype(jnp.bfloat16)
    arrived = lax.all_to_all(
        outbound.reshape(group, capacity, D), ("sp", "dp"), split_axis=0, concat_axis=0, tiled=True
    )
    flat_rows = arrived.reshape(group * capacity, D)
    produced = (
        swiglu_rows(flat_rows, gate_proj[0], up_proj[0], down_proj[0])
        .astype(jnp.bfloat16)
        .reshape(group, capacity, D)
    )
    returned = lax.all_to_all(produced, ("sp", "dp"), split_axis=0, concat_axis=0, tiled=True)
    returned_flat = returned.reshape(group * capacity, D)
    weights = route_weights[0]
    gates = weights / jnp.sum(weights, axis=-1, keepdims=True) * ROUTED
    routed = jnp.zeros((tok_rows, D), jnp.float32)
    for column in range(TOP_K):
        picker = (places[:, column : column + 1] == slot_ids[None, :]).astype(jnp.bfloat16)
        picked = jnp.dot(picker, returned_flat, preferred_element_type=jnp.float32)
        routed = routed + gates[:, column : column + 1] * picked
    feed = routed + swiglu_rows(first, shared_gate, shared_up, shared_down)
    result = layer_norm(ALPHA * first.astype(jnp.float32) + feed, norm2_gain, norm2_bias).astype(
        jnp.bfloat16
    )
    return result.reshape(1, tok_rows, D)


def solution(mesh):
    in_specs = (
        P("dp", "sp", None),
        P("dp", "sp", None),
        P("dp", "sp", None),
        P("dp", "sp", None),
        P(),
        P(),
        P(),
        P(),
        P(),
        P(),
        P("dp", "sp", None),
        P("dp", "sp", None),
        P(("sp", "dp"), None, None),
        P(("sp", "dp"), None, None),
        P(("sp", "dp"), None, None),
        P(),
        P(),
        P(),
        P(),
        P(),
    )
    out_specs = P("dp", "sp", None)
    return jax.shard_map(
        per_device, mesh=mesh, in_specs=in_specs, out_specs=out_specs, check_vma=False
    )
```

profile of v0, /device:TPU:0, one launch (start us, length us, event | category | flops | bytes accessed | tf_op | source)
XLA Modules:
  0.0 272.8 jit_solution(7604855050593937231)
XLA Ops:
  0.0 2.1 copy.65
  2.1 7.3 %all-to-all-start = ((bf16[128,8,192]{0,2,1:T(8,128)(2,1)}), bf16[128,8,192]{0,2,1:T(8,128)(2,1)S(1)}, u32[]{:S(2)}, u32[]{:S(2)}) async-start(bf16[128,8,192]{0,2,1:T(8,128)(2,1)} %bitcast.5), calls=%async_computation | async-start | bytes 786432 | tf_op jit(solution)/shard_map/all_to_all | solution.py:122
  9.4 0.8 copy.74
  10.4 1.0 fusion.28
  11.5 2.2 convolution_convert_fusion.3
  13.7 1.0 copy.79
  14.7 1.2 reduce-window.6
  16.3 27.6 %all_gather.3 = bf16[1024,32]{0,1:T(8,128)(2,1)} all-gather(bf16[128,32]{0,1:T(8,128)(2,1)S(1)} %pad_maximum_fusion), channel_id=1, replica_groups=mesh['sp'=8,'dp'=4] {'sp'}, dimensions={0}, use_global_device_ids=true | all-gather | bytes 73728 | tf_op jit(solution)/shard_map/all_gather | solution.py:125
  43.9 3.8 %all-to-all-start.1 = ((bf16[128,8,256]{0,2,1:T(8,128)(2,1)}), bf16[128,8,256]{0,2,1:T(8,128)(2,1)S(1)}, u32[]{:S(2)}, u32[]{:S(2)}) async-start(bf16[128,8,256]{0,2,1:T(8,128)(2,1)} %bitcast.11), calls=%async_computation.1 | async-start | bytes 1048576 | tf_op jit(solution)/shard_map/all_to_all | solution.py:123
  47.7 0.3 multiply_cosine_fusion
  48.0 1.0 copy.66
  49.0 1.2 reshape.192
  50.3 7.6 %all-to-all-done.1 = bf16[128,8,256]{0,2,1:T(8,128)(2,1)S(1)} async-done(((bf16[128,8,256]{0,2,1:T(8,128)(2,1)}), bf16[128,8,256]{0,2,1:T(8,128)(2,1)S(1)}, u32[]{:S(2)}, u32[]{:S(2)}) %all-to-all-start.1) | async-done | bytes 524320 | tf_op jit(solution)/shard_map/all_to_all | solution.py:123
  58.0 0.3 copy.68
  58.5 0.7 slice_bitcast_fusion
  59.3 0.8 broadcast_in_dim.14
  60.1 0.8 maximum_bitcast_fusion.1
  60.9 19.2 %while.22 = (s32[]{:T(128)}, bf16[2,1024,64]{2,1,0:T(8,128)(2,1)}, bf16[2,1024,96]{1,2,0:T(8,128)(2,1)S(1)}, bf16[2,1024,96]{1,2,0:T(8,128)(2,1)}, bf16[2,1024,6...) while((s32[]{:T(128)}, bf16[2,1024,64]{2,1,0:T(8,128)(2,1)}, ...), condition=%wide.region_6.7_spmd, body=%wide.region_1.6_spmd.sunk | while | flops 172523008 | bytes 9780014 | solution.py:143
  60.9 1.0 constant_dynamic-slice_fusion.5
  62.2 0.9 constant_dynamic-slice_fusion.6
  63.3 6.3 %while.23 = (s32[]{:T(128)}, bf16[2,512,64]{1,2,0:T(8,128)(2,1)S(1)}, s32[2]{0:T(128)S(1)}, bf16[2,512,96]{2,1,0:T(8,128)(2,1)S(1)}, bf16[1024,96]{1,0:T(8,128)(...) while((s32[]{:T(128)}, bf16[2,512,64]{1,2,0:T(8,128)(2,1)S(1)}, ...), condition=%wide.region_5.5_spmd.clone, body=%wide.region_2.4_spmd.clone.sunk | while | flops 172523008 | bytes 7026809 | solution.py:71
  63.3 0.7 dynamic_slice.37
  64.7 0.6 fusion.89
  65.3 0.5 fusion.90
  65.8 0.6 fusion.91
  66.5 0.7 dynamic_slice.37
  67.9 0.6 fusion.89
  68.4 0.5 fusion.90
  69.0 0.6 fusion.91
  69.8 0.7 bitcast_dynamic-update-slice_fusion.2
  70.5 1.0 constant_dynamic-slice_fusion.5
  71.8 0.9 constant_dynamic-slice_fusion.6
  72.9 6.3 %while.23 = (s32[]{:T(128)}, bf16[2,512,64]{1,2,0:T(8,128)(2,1)S(1)}, s32[2]{0:T(128)S(1)}, bf16[2,512,96]{2,1,0:T(8,128)(2,1)S(1)}, bf16[1024,96]{1,0:T(8,128)(...) while((s32[]{:T(128)}, bf16[2,512,64]{1,2,0:T(8,128)(2,1)S(1)}, ...), condition=%wide.region_5.5_spmd.clone, body=%wide.region_2.4_spmd.clone.sunk | while | flops 172523008 | bytes 7026809 | solution.py:71
  73.0 0.7 dynamic_slice.37
  74.3 0.6 fusion.89
  74.9 0.5 fusion.90
  75.4 0.6 fusion.91
  76.1 0.7 dynamic_slice.37
  77.5 0.6 fusion.89
  78.1 0.5 fusion.90
  78.6 0.6 fusion.91
  79.4 0.7 bitcast_dynamic-update-slice_fusion.2
  80.2 1.3 copy.72
  81.5 0.7 copy.73
  82.3 3.7 %all-to-all-start.2 = ((bf16[8,128,128]{1,2,0:T(8,128)(2,1)}), bf16[8,128,128]{1,2,0:T(8,128)(2,1)S(1)}, u32[]{:S(2)}, u32[]{:S(2)}) async-start(bf16[8,128,128]{1,2,0:T(8,128)(2,1)} %copy.73), calls=%async_computation.2 | async-start | bytes 524288 | tf_op jit(solution)/shard_map/all_to_all | solution.py:154
  86.5 7.7 %all-to-all-done.2 = bf16[8,128,128]{1,2,0:T(8,128)(2,1)S(1)} async-done(((bf16[8,128,128]{1,2,0:T(8,128)(2,1)}), bf16[8,128,128]{1,2,0:T(8,128)(2,1)S(1)}, u32[]{:S(2)}, u32[]{:S(2)}) %all-to-all-start.2) | async-done | bytes 262176 | tf_op jit(solution)/shard_map/all_to_all | solution.py:154
  94.6 3.0 %fusion.61 = (f32[128]{0:T(128)S(1)}, f32[128,2048]{1,0:T(8,128)S(1)}) fusion(bf16[128,1024]{0,1:T(8,128)(2,1)S(1)} %fusion.27, bf16[1024,2048]{1,0:T(8,128)(2,1)} %param.31, bf16[1,128,2048]{2,1,0:T(8,128)(2,1)S(1)} %copy-done.7), kind=kOutput, calls=%fused_computation.125 | convolution fusion | flops 537919360 | bytes 6029824 | tf_op jit(solution)/shard_map/dot_general | solution.py:156
  97.6 0.3 multiply_reduce_fusion.1
  97.9 0.2 add_convert_fusion.1
  98.1 1.0 convolution_convert_fusion.2
  99.1 73.9 %all_to_all.49 = bf16[32,24,2048]{2,1,0:T(8,128)(2,1)S(1)} all-to-all(bf16[32,24,2048]{2,1,0:T(8,128)(2,1)S(1)} %bitcast.157), channel_id=1, replica_groups=mesh['sp'=8,'dp'=4] {'sp','dp'}, dimensions={0} | all-to-all | bytes 6291456 | tf_op jit(solution)/shard_map/all_to_all | solution.py:170
  173.0 1.7 copy-done.2
  174.7 2.9 %fusion.16 = f32[768,512]{1,0:T(8,128)} fusion(bf16[768,2048]{1,0:T(8,128)(2,1)S(1)} %bitcast.162, bf16[1,2048,512]{2,1,0:T(8,128)(2,1)S(1)} %copy-done.16), kind=kOutput, calls=%fused_computation.33 | convolution fusion | flops 1610612736 | bytes 6815744 | tf_op jit(solution)/shard_map/dot_general | solution.py:76
  177.6 8.1 %convolution_convert_fusion.1 = bf16[768,2048]{1,0:T(8,128)(2,1)} fusion(bf16[1,512,2048]{2,1,0:T(8,128)(2,1)S(1)} %copy-done, f32[768,512]{1,0:T(8,128)} %fusion.16, bf16[768,2048]{1,0:T(8,128)(2,1)} %bitcast.163, bf16[1,2048,512]{2,1,0:T(8,128)(2,1)} %param.37), kind=kOutput, calls=%fused_computation.17 | convolution fusion | flops 3225157632 | bytes 12058624 | tf_op jit(solution)/shard_map/dot_general | solution.py:79
  185.8 3.8 %all-to-all-start.4 = ((bf16[32,24,2048]{2,1,0:T(8,128)(2,1)}), bf16[32,24,2048]{2,1,0:T(8,128)(2,1)}, u32[]{:S(2)}, u32[]{:S(2)}) async-start(bf16[32,24,2048]{2,1,0:T(8,128)(2,1)} %bitcast.161), calls=%async_computation.4 | async-start | bytes 6291456 | tf_op jit(solution)/shard_map/all_to_all | solution.py:179
  189.9 2.0 fusion.63
  192.0 4.1 %fusion.22 = f32[128,2048]{1,0:T(8,128)} fusion(bf16[512,2048]{1,0:T(8,128)(2,1)} %param.41, bf16[128,2048]{1,0:T(8,128)(2,1)S(1)} %add_convert_fusion.1, bf16[2048,512]{1,0:T(8,128)(2,1)} %param.40, f32[128,512]{1,0:T(8,128)S(1)} %fusion.63), kind=kOutput, calls=%fused_computation.40 | convolution fusion | flops 537264128 | bytes 6029312 | tf_op jit(solution)/shard_map/dot_general | solution.py:79
  196.1 64.8 %all-to-all-done.4 = bf16[32,24,2048]{2,1,0:T(8,128)(2,1)} async-done(((bf16[32,24,2048]{2,1,0:T(8,128)(2,1)}), bf16[32,24,2048]{2,1,0:T(8,128)(2,1)}, u32[]{:S(2)}, u32[]{:S(2)}) %all-to-all-start.4) | async-done | bytes 3145760 | tf_op jit(solution)/shard_map/all_to_all | solution.py:179
  260.9 2.5 convolution_multiply_fusion.1
  263.4 2.5 convolution_multiply_fusion.2
  265.9 2.6 convolution_multiply_fusion
  268.5 3.0 %fusion.62 = (f32[128]{0:T(128)S(1)}, f32[128,2048]{1,0:T(8,128)S(1)}) fusion(f32[128,2048]{1,0:T(8,128)S(1)} %copy-done.1, f32[128,2048]{1,0:T(8,128)S(1)} %convolution_multiply_fusion, f32[128,2048]{1,0:T(8,128)S(1)} %convolution_multiply_fusion.1, f32[128,2048]{1,0:T(8,128)S(1)} %convolution_multiply_fusion.2, bf16[768,2048]{1,0:T(8,128)(2,1)} %bitcast.33, ...), kind=kOutput, calls=%fused_computation.126 | convolution fusion | flops 405110656 | bytes 8914432 | tf_op jit(solution)/shard_map/dot_general | solution.py:186
  271.5 0.3 multiply_reduce_fusion
  271.8 1.0 fusion.25
  (89 shorter events, 3.8 us)
Async XLA Ops:
  0.0 177.6 %copy-start = (bf16[1,512,2048]{2,1,0:T(8,128)(2,1)S(1)}, bf16[1,512,2048]{2,1,0:T(8,128)(2,1)}, u32[]{:S(2)}) copy-start(bf16[1,512,2048]{2,1,0:T(8,128)(2,1)} %param.38) | copy-start | bytes 6291460
  2.1 41.8 %all-to-all-start = ((bf16[128,8,192]{0,2,1:T(8,128)(2,1)}), bf16[128,8,192]{0,2,1:T(8,128)(2,1)S(1)}, u32[]{:S(2)}, u32[]{:S(2)}) async-start(bf16[128,8,192]{0,2,1:T(8,128)(2,1)} %bitcast.5), calls=%async_computation | async-start | bytes 786432 | tf_op jit(solution)/shard_map/all_to_all | solution.py:122
  10.2 1.3 copy-start.3
  10.4 5.7 %copy-start.13 = (bf16[1,128,32]{1,2,0:T(8,128)(2,1)S(1)}, bf16[1,128,32]{1,2,0:T(8,128)(2,1)}, u32[]{:S(2)}) copy-start(bf16[1,128,32]{1,2,0:T(8,128)(2,1)} %param.27) | copy-start | bytes 24580
  15.8 32.1 %copy-start.5 = (s32[32,4,128]{2,0,1:T(8,128)}, s32[32,4,128]{2,0,1:T(8,128)S(1)}, u32[]{:S(2)}) copy-start(s32[32,4,128]{2,0,1:T(8,128)S(1)} %reduce-window.6) | copy-start | bytes 196612
  16.1 34.2 %copy-start.8 = (s32[32,5]{0,1:T(8,128)}, s32[32,5]{0,1:T(8,128)S(1)}, u32[]{:S(2)}) copy-start(s32[32,5]{0,1:T(8,128)S(1)} %reduce-window.9) | copy-start | bytes 1924
  43.9 14.1 %all-to-all-start.1 = ((bf16[128,8,256]{0,2,1:T(8,128)(2,1)}), bf16[128,8,256]{0,2,1:T(8,128)(2,1)S(1)}, u32[]{:S(2)}, u32[]{:S(2)}) async-start(bf16[128,8,256]{0,2,1:T(8,128)(2,1)} %bitcast.11), calls=%async_computation.1 | async-start | bytes 1048576 | tf_op jit(solution)/shard_map/all_to_all | solution.py:123
  80.1 5.8 %copy-start.6 = (s32[32,4,128]{2,0,1:T(8,128)S(1)}, s32[32,4,128]{2,0,1:T(8,128)}, u32[]{:S(2)}) copy-start(s32[32,4,128]{2,0,1:T(8,128)} %copy-done.5) | copy-start | bytes 196612
  80.1 5.8 %slice-start = ((s32[32,5]{0,1:T(8,128)}), s32[32,4]{0,1:T(4,128)S(1)}, s32[]{:S(2)}) async-start(s32[32,5]{0,1:T(8,128)} %copy-done.8), calls=%async_computation.5 | async-start | bytes 4096 | tf_op jit(solution)/shard_map/slice.1
  80.1 6.0 %copy-start.4 = (s32[1,128,4]{2,1,0:T(8,128)S(1)}, s32[1,128,4]{2,1,0:T(8,128)}, u32[]{:S(2)}) copy-start(s32[1,128,4]{2,1,0:T(8,128)} %copy-done.3) | copy-start | bytes 6148
  80.1 14.2 %copy-start.15 = (f32[1024]{0:T(1024)S(1)}, f32[1024]{0:T(1024)}, u32[]{:S(2)}) copy-start(f32[1024]{0:T(1024)} %param.30) | copy-start | bytes 12292
  80.1 14.4 %copy-start.7 = (bf16[1,128,2048]{2,1,0:T(8,128)(2,1)S(1)}, bf16[1,128,2048]{2,1,0:T(8,128)(2,1)}, u32[]{:S(2)}) copy-start(bf16[1,128,2048]{2,1,0:T(8,128)(2,1)} %param.24) | copy-start | bytes 1572868
  82.3 11.9 %all-to-all-start.2 = ((bf16[8,128,128]{1,2,0:T(8,128)(2,1)}), bf16[8,128,128]{1,2,0:T(8,128)(2,1)S(1)}, u32[]{:S(2)}, u32[]{:S(2)}) async-start(bf16[8,128,128]{1,2,0:T(8,128)(2,1)} %copy.73), calls=%async_computation.2 | async-start | bytes 524288 | tf_op jit(solution)/shard_map/all_to_all | solution.py:154
  94.5 3.3 %copy-start.9 = (f32[2048]{0:T(1024)S(1)}, f32[2048]{0:T(1024)}, u32[]{:S(2)}) copy-start(f32[2048]{0:T(1024)} %param.33) | copy-start | bytes 24580
  94.6 3.3 %copy-start.10 = (f32[2048]{0:T(1024)S(1)}, f32[2048]{0:T(1024)}, u32[]{:S(2)}) copy-start(f32[2048]{0:T(1024)} %param.32) | copy-start | bytes 24580
  99.1 75.6 %copy-start.16 = (bf16[1,2048,512]{2,1,0:T(8,128)(2,1)S(1)}, bf16[1,2048,512]{2,1,0:T(8,128)(2,1)}, u32[]{:S(2)}) copy-start(bf16[1,2048,512]{2,1,0:T(8,128)(2,1)} %param.36) | copy-start | bytes 6291460
  173.0 1.7 copy-start.2
  185.8 3.9 %copy-start.14 = (f32[1,128,4]{1,2,0:T(4,128)S(1)}, f32[1,128,4]{1,2,0:T(4,128)}, u32[]{:S(2)}) copy-start(f32[1,128,4]{1,2,0:T(4,128)} %param.35) | copy-start | bytes 6148
  185.8 75.1 %all-to-all-start.4 = ((bf16[32,24,2048]{2,1,0:T(8,128)(2,1)}), bf16[32,24,2048]{2,1,0:T(8,128)(2,1)}, u32[]{:S(2)}, u32[]{:S(2)}) async-start(bf16[32,24,2048]{2,1,0:T(8,128)(2,1)} %bitcast.161), calls=%async_computation.4 | async-start | bytes 6291456 | tf_op jit(solution)/shard_map/all_to_all | solution.py:179
  265.9 2.6 copy-start.1
  268.5 3.3 %copy-start.11 = (f32[2048]{0:T(1024)S(1)}, f32[2048]{0:T(1024)}, u32[]{:S(2)}) copy-start(f32[2048]{0:T(1024)} %param.43) | copy-start | bytes 24580
  268.5 3.3 %copy-start.12 = (f32[2048]{0:T(1024)S(1)}, f32[2048]{0:T(1024)}, u32[]{:S(2)}) copy-start(f32[2048]{0:T(1024)} %param.42) | copy-start | bytes 24580
where the time goes:
time: 274 us; the launch traced here: 273 us
  blocking collectives  101 us (37%)
  waiting for transfers between devices  80.1 us (29%)
  matrix products  38.8 us (14%)
  local copies, waits for them, and re-layouts  22.2 us (8%)
  starting transfers between devices  18.5 us (7%)
  other arithmetic  8.2 us (3%)
  loops' own time  3.02 us (1%)
    all_to_all x1, blocking collectives, per_device(): lax.all_to_all(outbound.reshape(group, capacity, D), ('sp', 'dp'), split_...  73.9 us
    all_to_all x1, waiting for transfers between devices, per_device(): lax.all_to_all(produced, ('sp', 'dp'), split_axis=0, concat_axis=0, tiled...  64.8 us
    all_gather x1, blocking collectives, per_device(): keys_whole = lax.all_gather(keys_turned, 'sp', axis=0, tiled=True)  27.6 us
    dot_general x2, matrix products, swiglu_rows(): return jnp.dot(inner, down_mat, preferred_element_type=jnp.float32)  12.2 us
    dot_general x4, matrix products, per_device(): picked = jnp.dot(picker, returned_flat, preferred_element_type=jnp.float32)  10.6 us
    all_to_all x1, waiting for transfers between devices, per_device(): lax.all_to_all(outgoing, 'sp', split_axis=0, concat_axis=2, tiled=True)  7.66 us
    all_to_all x1, waiting for transfers between devices, per_device(): lax.all_to_all(pair_send, 'sp', split_axis=1, concat_axis=0, tiled=True)  7.63 us
    all_to_all x1, starting transfers between devices, per_device(): lax.all_to_all(query_send, 'sp', split_axis=1, concat_axis=0, tiled=True)  7.31 us
  transfers between devices with their start and end apart: 4, of which 3 were waited for; matrix products, arithmetic and copies ran while one was open for 6% of the time, Pallas kernels for 0%

commit v1 on v0

--- a/solution.py
+++ b/solution.py
@@ -1,8 +1,11 @@
+import functools
 import math
 
 import jax
 import jax.numpy as jnp
 from jax import lax
+from jax.experimental import pallas as pl
+from jax.experimental.pallas import tpu as pltpu
 from jax.sharding import PartitionSpec as P
 
 D = 2048
@@ -50,26 +53,135 @@
     )
 
 
-def attend(query, key_full, values):
-    length = query.shape[0]
-    span_rows = 512
-    block_count = length // span_rows
-    blocks = query.reshape(block_count, span_rows, query.shape[1])
-    key_pos = jnp.arange(length, dtype=jnp.int32)
-    factor = 1.0 / math.sqrt(query.shape[1])
-
-    def one_block(inputs):
-        block_index, query_rows = inputs
-        scores = jnp.dot(query_rows, key_full.T, preferred_element_type=jnp.float32) * factor
-        query_pos = block_index * span_rows + jnp.arange(span_rows, dtype=jnp.int32)
-        scores = jnp.where(key_pos[None, :] <= query_pos[:, None], scores, -jnp.inf)
+MESH = pl.DeviceIdType.MESH
+LANES = 128
+
+
+def inner_of(count):
+    return count // 4 if count % 4 == 0 else 1
+
+
+def gather_kernel(count, x_ref, out_ref, own_sem, send_sem, recv_sem):
+    inner = inner_of(count)
+    outer = count // inner
+    me = lax.axis_index("sp")
+    far, near = me // inner, me % inner
+    far_peers = [((far + step) % outer) * inner + near for step in range(1, outer)]
+    near_peers = [far * inner + (near + step) % inner for step in range(1, inner)]
+
+    barrier = pltpu.get_barrier_semaphore()
+    for peer in far_peers + near_peers:
+        pl.semaphore_signal(barrier, inc=1, device_id={"sp": peer}, device_id_type=MESH)
+    pl.semaphore_wait(barrier, len(far_peers) + len(near_peers))
+
+    started = []
+
+    def send(source, owner, peer):
+        copy = pltpu.make_async_remote_copy(
+            src_ref=source,
+            dst_ref=out_ref.at[owner],
+            send_sem=send_sem.at[len(started)],
+            recv_sem=recv_sem.at[owner],
+            device_id={"sp": peer},
+            device_id_type=MESH,
+        )
+        copy.start()
+        started.append(copy)
+
+    def arrive(owner):
+        pltpu.make_async_remote_copy(
+            src_ref=x_ref,
+            dst_ref=out_ref.at[owner],
+            send_sem=send_sem.at[0],
+            recv_sem=recv_sem.at[owner],
+            device_id={"sp": (me + 1) % count},
+            device_id_type=MESH,
+        ).wait_recv()
+
+    for peer in far_peers + near_peers:
+        send(x_ref, me, peer)
+    own = pltpu.make_async_copy(x_ref, out_ref.at[me], own_sem)
+    own.start()
+    for step in range(1, outer):
+        owner = ((far + outer - step) % outer) * inner + near
+        arrive(owner)
+        for peer in near_peers:
+            send(out_ref.at[owner], owner, peer)
+    for other in range(1, inner):
+        for step in range(outer):
+            arrive(((far + outer - step) % outer) * inner + (near + inner - other) % inner)
+    own.wait()
+    for copy in started:
+        copy.wait_send()
+
+
+def gather_rows(block):
+    count = lax.axis_size("sp")
+    inner = inner_of(count)
+    outer = count // inner
+    sends = (outer - 1) + (inner - 1) * outer
+    rows, width = block.shape
+    return pl.pallas_call(
+        functools.partial(gather_kernel, count),
+        out_shape=jax.ShapeDtypeStruct((count, rows, width), block.dtype),
+        in_specs=[pl.BlockSpec(memory_space=pltpu.VMEM)],
+        out_specs=pl.BlockSpec(memory_space=pltpu.VMEM),
+        scratch_shapes=[
+            pltpu.SemaphoreType.DMA,
+            pltpu.SemaphoreType.DMA((sends,)),
+            pltpu.SemaphoreType.DMA((count,)),
+        ],
+        compiler_params=pltpu.CompilerParams(collective_id=0, has_side_effects=True),
+    )(block).reshape(count * rows, width)
+
+
+PAIR = 2
+
+
+def attend_kernel(offset_ref, query_ref, whole_ref, up_ref, out_ref):
+    rows = query_ref.shape[2]
+    latent_width = up_ref.shape[0]
+    length = whole_ref.shape[0]
+    head_width = PLAIN_HEAD_WIDTH + VALUE_HEAD_WIDTH
+    factor = math.log2(math.e) / math.sqrt(PLAIN_HEAD_WIDTH + QK_ROPE)
+    latents = whole_ref[:, :latent_width]
+    turned = whole_ref[:, latent_width:]
+    pairs = jnp.dot(latents, up_ref[...], preferred_element_type=jnp.float32).astype(jnp.bfloat16)
+    query_pos = offset_ref[0] + lax.broadcasted_iota(jnp.int32, (rows, length), 0)
+    visible = lax.broadcasted_iota(jnp.int32, (rows, length), 1) <= query_pos
+    outs = []
+    for head in range(PAIR):
+        block = pairs[:, head * head_width : (head + 1) * head_width]
+        keys = jnp.concatenate([block, turned], axis=1)
+        scores = lax.dot_general(
+            query_ref[0, head], keys, (((1,), (1,)), ((), ())), preferred_element_type=jnp.float32
+        )
+        scores = jnp.where(visible, scores, -jnp.inf)
         row_max = jnp.max(scores, axis=-1, keepdims=True)
-        weights = jnp.exp(scores - row_max)
-        weights = (weights / jnp.sum(weights, axis=-1, keepdims=True)).astype(jnp.bfloat16)
-        return jnp.dot(weights, values, preferred_element_type=jnp.float32).astype(jnp.bfloat16)
-
-    attended = lax.map(one_block, (jnp.arange(block_count, dtype=jnp.int32), blocks))
-    return attended.reshape(length, values.shape[1])
+        weights = jnp.exp2((scores - row_max) * factor)
+        total = jnp.sum(weights, axis=-1, keepdims=True)
+        mixed = jnp.dot(weights.astype(jnp.bfloat16), block, preferred_element_type=jnp.float32)
+        outs.append((mixed / total)[:, PLAIN_HEAD_WIDTH:])
+    out_ref[...] = jnp.concatenate(outs, axis=1).astype(out_ref.dtype)
+
+
+def attend(query_full, whole, up_weight, offset):
+    rows = query_full.shape[1]
+    steps = ATTENTION_HEADS // PAIR
+    span = PAIR * (PLAIN_HEAD_WIDTH + VALUE_HEAD_WIDTH)
+    width = query_full.shape[2]
+    return pl.pallas_call(
+        attend_kernel,
+        grid=(steps,),
+        out_shape=jax.ShapeDtypeStruct((rows, ATTENTION_HEADS * VALUE_HEAD_WIDTH), jnp.bfloat16),
+        in_specs=[
+            pl.BlockSpec(memory_space=pltpu.SMEM),
+            pl.BlockSpec((1, PAIR, rows, width), lambda step: (step, 0, 0, 0)),
+            pl.BlockSpec(whole.shape, lambda step: (0, 0)),
+            pl.BlockSpec((up_weight.shape[0], span), lambda step: (0, step)),
+        ],
+        out_specs=pl.BlockSpec((rows, PAIR * VALUE_HEAD_WIDTH), lambda step: (0, step)),
+    )(offset, query_full.reshape(steps, PAIR, rows, width), whole, up_weight)
 
 
 def swiglu_rows(rows, gate_mat, up_mat, down_mat):
@@ -101,58 +213,34 @@
     norm2_gain,
     norm2_bias,
 ):
-    seq_devices = lax.axis_size("sp")
     tok_rows = hidden_in.shape[1]
-    length = tok_rows * seq_devices
-    heads_here = ATTENTION_HEADS // seq_devices
     normed = rms_scaled(key_value_latent[0], latent_norm_gain).astype(jnp.bfloat16)
-    keys_values = jnp.dot(normed, latent_up_weight, preferred_element_type=jnp.float32).astype(
-        jnp.bfloat16
-    )
-    local_pos = lax.axis_index("sp") * tok_rows + jnp.arange(tok_rows, dtype=jnp.int32)
+    start = lax.axis_index("sp") * tok_rows
+    local_pos = start + jnp.arange(tok_rows, dtype=jnp.int32)
     cos_local, sin_local = rotation_tables(local_pos, QK_ROPE)
     keys_turned = turn(keys_rope[0].astype(jnp.float32), cos_local, sin_local).astype(jnp.bfloat16)
-    query_send = queries[0].reshape(
-        tok_rows, seq_devices, heads_here * (PLAIN_HEAD_WIDTH + QK_ROPE)
-    )
-    pair_send = keys_values.reshape(
-        tok_rows, seq_devices, heads_here * (PLAIN_HEAD_WIDTH + VALUE_HEAD_WIDTH)
-    )
-    query_heads, pair_heads = (
-        lax.all_to_all(query_send, "sp", split_axis=1, concat_axis=0, tiled=True),
-        lax.all_to_all(pair_send, "sp", split_axis=1, concat_axis=0, tiled=True),
-    )
-    keys_whole = lax.all_gather(keys_turned, "sp", axis=0, tiled=True)
-    query_heads = query_heads.reshape(length, heads_here, PLAIN_HEAD_WIDTH + QK_ROPE)
-    pair_heads = pair_heads.reshape(length, heads_here, PLAIN_HEAD_WIDTH + VALUE_HEAD_WIDTH)
-    cos_whole, sin_whole = rotation_tables(jnp.arange(length, dtype=jnp.int32), QK_ROPE)
+    whole = gather_rows(
+        jnp.concatenate([normed, jnp.pad(keys_turned, ((0, 0), (0, LANES - QK_ROPE)))], axis=1)
+    )
+    query_heads = queries[0].reshape(tok_rows, ATTENTION_HEADS, PLAIN_HEAD_WIDTH + QK_ROPE)
     query_turned = turn(
         query_heads[..., PLAIN_HEAD_WIDTH:].astype(jnp.float32),
-        cos_whole[:, None, :],
-        sin_whole[:, None, :],
+        cos_local[:, None, :],
+        sin_local[:, None, :],
     ).astype(jnp.bfloat16)
-    query_full = jnp.concatenate([query_heads[..., :PLAIN_HEAD_WIDTH], query_turned], axis=-1)
-    key_full = jnp.concatenate(
+    query_full = jnp.concatenate(
         [
-            pair_heads[..., :PLAIN_HEAD_WIDTH],
-            jnp.broadcast_to(keys_whole[:, None, :], (length, heads_here, QK_ROPE)),
+            query_heads[..., :PLAIN_HEAD_WIDTH],
+            jnp.zeros((tok_rows, ATTENTION_HEADS, VALUE_HEAD_WIDTH), jnp.bfloat16),
+            query_turned,
+            jnp.zeros((tok_rows, ATTENTION_HEADS, LANES - QK_ROPE), jnp.bfloat16),
         ],
         axis=-1,
     )
-    values_heads = pair_heads[..., PLAIN_HEAD_WIDTH:]
-    by_head = lax.map(
-        lambda inputs: attend(inputs[0], inputs[1], inputs[2]),
-        (
-            jnp.moveaxis(query_full, 1, 0),
-            jnp.moveaxis(key_full, 1, 0),
-            jnp.moveaxis(values_heads, 1, 0),
-        ),
-    )
-    outgoing = jnp.moveaxis(by_head, 0, 1).reshape(
-        seq_devices, tok_rows, heads_here * VALUE_HEAD_WIDTH
-    )
-    incoming = lax.all_to_all(outgoing, "sp", split_axis=0, concat_axis=2, tiled=True)
-    attn_normed = rms_scaled(incoming[0], attn_gain).astype(jnp.bfloat16)
+    attended = attend(
+        jnp.moveaxis(query_full, 1, 0), whole, latent_up_weight, start.reshape(1).astype(jnp.int32)
+    )
+    attn_normed = rms_scaled(attended, attn_gain).astype(jnp.bfloat16)
     mixed = jnp.dot(attn_normed, out_proj, preferred_element_type=jnp.float32)
     first = layer_norm(
         ALPHA * hidden_in[0].astype(jnp.float32) + mixed, norm1_gain, norm1_bias

time: 274 us -> 245 us (0.89)
  Pallas kernels: 0 us -> 43.9 us
  blocking collectives: 101 us -> 77.1 us
  waiting for transfers between devices: 80.1 us -> 64.7 us
  starting transfers between devices: 18.5 us -> 3.98 us
  local copies, waits for them, and re-layouts: 22.2 us -> 13.4 us
  matrix products: 38.8 us -> 31.9 us
  loops' own time: 3.02 us -> 0 us
    pallas_call x0 -> x2, Pallas kernels: none -> 43.9 us  [the longest x1 28.1 us: gather_rows(): pl.pallas_call(functools.partial(gather_kernel, count), out_shape=jax.Sha...]
    all_gather x1 -> x0, blocking collectives: 27.6 us -> none  [per_device(): keys_whole = lax.all_gather(keys_turned, 'sp', axis=0, tiled=True)]
    all_to_all x3 -> x0, waiting for transfers between devices: 15.3 us -> none  [the longest x1 7.66 us: per_device(): lax.all_to_all(outgoing, 'sp', split_axis=0, concat_axis=2, tiled=True)]
    all_to_all x3 -> x0, starting transfers between devices: 14.8 us -> none  [the longest x1 7.31 us: per_device(): lax.all_to_all(query_send, 'sp', split_axis=1, concat_axis=0, tiled=True)]
    dynamic_slice x14 -> x0, local copies, waits for them, and re-layouts: 7.42 us -> none  [the longest x10 4.76 us: per_device(): lax.map(lambda inputs: attend(inputs[0], inputs[1], inputs[2]), (jnp.move...]
    dot_general x9 -> x0, matrix products: 7.11 us -> none  [the longest x4 2.56 us: one_block(): jnp.dot(weights, values, preferred_element_type=jnp.float32)]
    concatenate x0 -> x2, local copies, waits for them, and re-layouts: none -> 4.09 us  [the longest x1 3.96 us: per_device(): jnp.concatenate([query_heads[..., :PLAIN_HEAD_WIDTH], jnp.zeros((tok_rows...]
    all_to_all x1, blocking collectives: 73.9 us -> 77.1 us  [per_device(): lax.all_to_all(outbound.reshape(group, capacity, D), ('sp', 'dp'), split_...]
  transfers between devices with their start and end apart: 4 -> 1, of which waited for: 3 -> 1; matrix products, arithmetic and copies ran while one was open for 6% -> 3% of each run, Pallas kernels for 0% -> 0%
where the time goes in v1:
time: 245 us
  blocking collectives  77.1 us (31%)
  waiting for transfers between devices  64.7 us (26%)
  Pallas kernels  43.9 us (18%)
  matrix products  31.9 us (13%)
  local copies, waits for them, and re-layouts  13.4 us (5%)
  other arithmetic  9.36 us (4%)
  starting transfers between devices  3.98 us (2%)
    all_to_all x1, blocking collectives, per_device(): lax.all_to_all(outbound.reshape(group, capacity, D), ('sp', 'dp'), split_...  77.1 us
    all_to_all x1, waiting for transfers between devices, per_device(): lax.all_to_all(produced, ('sp', 'dp'), split_axis=0, concat_axis=0, tiled...  64.7 us
    pallas_call x1, Pallas kernels, gather_rows(): pl.pallas_call(functools.partial(gather_kernel, count), out_shape=jax.Sha...  28.1 us
    pallas_call x1, Pallas kernels, attend(): pl.pallas_call(attend_kernel, grid=(steps,), out_shape=jax.ShapeDtypeStru...  15.8 us
    dot_general x2, matrix products, swiglu_rows(): return jnp.dot(inner, down_mat, preferred_element_type=jnp.float32)  12.2 us
    dot_general x4, matrix products, per_device(): picked = jnp.dot(picker, returned_flat, preferred_element_type=jnp.float32)  10.6 us
    dot_general x2, matrix products, swiglu_rows(): gated = jnp.dot(rows, gate_mat, preferred_element_type=jnp.float32)  4.96 us
  transfers between devices with their start and end apart: 1, of which 1 were waited for; matrix products, arithmetic and copies ran while one was open for 3% of the time, Pallas kernels for 0%

profile of v1, /device:TPU:0, one launch (start us, length us, event | category | flops | bytes accessed | tf_op | source)
XLA Modules:
  0.0 244.6 jit_solution(10553107734522686119)
XLA Ops:
  0.0 0.0 copy-start
  0.0 1.4 copy.56
  1.4 0.8 copy.61
  2.2 0.1 eq.104
  2.3 0.1 eq.100
  2.5 0.7 bitcast_convert_fusion
  3.2 0.1 subtract_convert_fusion.1
  3.3 0.3 copy.58
  3.6 0.3 copy.59
  3.9 1.0 copy.57
  4.9 0.1 copy.60
  5.1 1.0 fusion.22
  6.1 1.0 fusion.24
  7.1 0.7 fusion.37.x_ref
  7.8 28.1 %shard_map.190 = bf16[8,128,640]{2,1,0:T(8,128)(2,1)} custom-call(bf16[128,640]{1,0:T(8,128)(2,1)} %fusion.37.x_ref), custom_call_target="tpu_custom_call" | custom-call | tf_op jit(solution)/shard_map/pallas_call | solution.py:124
  35.9 0.9 broadcast_in_dim.4
  36.8 0.9 broadcast_in_dim.5
  37.7 4.0 %concatenate.13 = bf16[128,16,256]{2,0,1:T(8,128)(2,1)} concatenate(bf16[128,16,64]{2,0,1:T(8,128)(2,1)} %copy.57, bf16[128,16,64]{2,0,1:T(8,128)(2,1)} %broadcast_in_dim.4, bf16[128,16,16]{2,0,1:T(8,128)(2,1)S(1)} %copy.58, bf16[128,16,16]{2,0,1:T(8,128)(2,1)S(1)} %copy.59, bf16[128,16,96]{2,0,1:T(8,128)(2,1)} %broadcast_in_dim.5), dimensions={2} | concatenate | bytes 2097152 | tf_op jit(solution)/shard_map/concatenate | solution.py:231
  41.7 15.8 %shard_map.191 = bf16[128,1024]{1,0:T(8,128)(2,1)} custom-call(s32[1]{0:T(128)} %bitcast.1.offset_ref, bf16[8,2,128,256]{3,2,1,0:T(8,128)(2,1)} %bitcast.85, bf16[1024,640]{1,0:T(8,128)(2,1)} %bitcast.84, bf16[512,2048]{1,0:T(8,128)(2,1)} %up_ref.1), custom_call_target="tpu_custom_call" | custom-call | tf_op jit(solution)/shard_map/pallas_call | solution.py:173
  57.5 1.1 fusion.17
  58.6 0.0 copy-done.4
  58.6 0.0 copy-done.10
  58.6 0.0 copy-start.5
  58.6 0.0 copy-start.6
  58.6 3.2 %fusion.46 = (f32[128]{0:T(128)S(1)}, f32[128,2048]{1,0:T(8,128)S(1)}) fusion(bf16[1024,2048]{1,0:T(8,128)(2,1)} %param.27, bf16[128,1024]{1,0:T(8,128)(2,1)} %shard_map.191, f32[1024]{0:T(1024)S(1)} %copy-done.10, f32[128]{0:T(128)S(1)} %add_rsqrt_fusion.2, bf16[1,128,2048]{2,1,0:T(8,128)(2,1)S(1)} %copy-done.4), kind=kOutput, calls=%fused_computation.97 | convolution fusion | flops 538443648 | bytes 6034432 | tf_op jit(solution)/shard_map/dot_general | solution.py:244
  61.8 0.0 copy-start.1
  61.8 1.0 copy-done.1
  62.8 0.3 multiply_reduce_fusion.1
  63.1 1.2 reduce-window.6
  64.3 0.2 slice_reduce_fusion.4
  64.5 0.1 fusion.41
  64.6 0.1 reduce_sum.83
  64.8 0.1 copy.65
  64.8 0.2 fusion.10
  65.1 0.0 copy-done.5
  65.1 0.0 copy-done.6
  65.1 1.5 add_convert_fusion.1
  66.6 1.0 convolution_convert_fusion.1
  67.5 0.0 copy-start.11
  67.6 77.1 %all_to_all.10 = bf16[32,24,2048]{2,1,0:T(8,128)(2,1)S(1)} all-to-all(bf16[32,24,2048]{2,1,0:T(8,128)(2,1)S(1)} %bitcast.83), channel_id=1, replica_groups=mesh['sp'=8,'dp'=4] {'sp','dp'}, dimensions={0} | all-to-all | bytes 6291456 | tf_op jit(solution)/shard_map/all_to_all | solution.py:258
  144.7 1.7 copy-done.3
  146.4 0.0 copy-done.11
  146.4 2.9 %fusion.8 = f32[768,512]{1,0:T(8,128)} fusion(bf16[768,2048]{1,0:T(8,128)(2,1)S(1)} %bitcast.87, bf16[1,2048,512]{2,1,0:T(8,128)(2,1)S(1)} %copy-done.11), kind=kOutput, calls=%fused_computation.15 | convolution fusion | flops 1610612736 | bytes 6815744 | tf_op jit(solution)/shard_map/dot_general | solution.py:188
  149.3 0.0 copy-done
  149.3 8.1 %convolution_convert_fusion = bf16[768,2048]{1,0:T(8,128)(2,1)} fusion(bf16[1,512,2048]{2,1,0:T(8,128)(2,1)S(1)} %copy-done, f32[768,512]{1,0:T(8,128)} %fusion.8, bf16[768,2048]{1,0:T(8,128)(2,1)} %bitcast.88, bf16[1,2048,512]{2,1,0:T(8,128)(2,1)} %param.33), kind=kOutput, calls=%fused_computation | convolution fusion | flops 3225157632 | bytes 12058624 | tf_op jit(solution)/shard_map/dot_general | solution.py:191
  157.4 4.0 %all-to-all-start.1 = ((bf16[32,24,2048]{2,1,0:T(8,128)(2,1)}), bf16[32,24,2048]{2,1,0:T(8,128)(2,1)}, u32[]{:S(2)}, u32[]{:S(2)}) async-start(bf16[32,24,2048]{2,1,0:T(8,128)(2,1)} %bitcast.86), calls=%async_computation.1 | async-start | bytes 6291456 | tf_op jit(solution)/shard_map/all_to_all | solution.py:267
  161.4 0.1 reduce_sum.82
  161.5 0.0 copy-done.9
  161.6 0.2 slice_reduce_fusion.3
  161.8 2.0 fusion.48
  163.9 4.1 %fusion.14 = f32[128,2048]{1,0:T(8,128)} fusion(bf16[512,2048]{1,0:T(8,128)(2,1)} %param.37, bf16[128,2048]{1,0:T(8,128)(2,1)S(1)} %add_convert_fusion.1, bf16[2048,512]{1,0:T(8,128)(2,1)} %param.36, f32[128,512]{1,0:T(8,128)S(1)} %fusion.48), kind=kOutput, calls=%fused_computation.22 | convolution fusion | flops 537264128 | bytes 6029312 | tf_op jit(solution)/shard_map/dot_general | solution.py:191
  167.9 64.7 %all-to-all-done.1 = bf16[32,24,2048]{2,1,0:T(8,128)(2,1)} async-done(((bf16[32,24,2048]{2,1,0:T(8,128)(2,1)}), bf16[32,24,2048]{2,1,0:T(8,128)(2,1)}, u32[]{:S(2)}, u32[]{:S(2)}) %all-to-all-start.1) | async-done | bytes 3145760 | tf_op jit(solution)/shard_map/all_to_all | solution.py:267
  232.7 2.5 %convolution_multiply_fusion.1 = f32[128,2048]{1,0:T(8,128)S(1)} fusion(bf16[768,2048]{1,0:T(8,128)(2,1)} %bitcast.21, f32[128]{0:T(128)S(1)} %get-tuple-element.15, s32[128]{0:T(128)S(1)} %get-tuple-element.7), kind=kOutput, calls=%fused_computation.3 | convolution fusion | flops 403013632 | bytes 4195328 | tf_op jit(solution)/shard_map/dot_general | solution.py:274
  235.2 2.5 %convolution_multiply_fusion.2 = f32[128,2048]{1,0:T(8,128)S(1)} fusion(bf16[768,2048]{1,0:T(8,128)(2,1)} %bitcast.21, f32[128]{0:T(128)S(1)} %get-tuple-element.16, s32[128]{0:T(128)S(1)} %get-tuple-element.8), kind=kOutput, calls=%fused_computation.4 | convolution fusion | flops 403013632 | bytes 4195328 | tf_op jit(solution)/shard_map/dot_general | solution.py:274
  237.7 0.0 copy-start.2
  237.7 2.6 %convolution_multiply_fusion = f32[128,2048]{1,0:T(8,128)S(1)} fusion(bf16[768,2048]{1,0:T(8,128)(2,1)} %bitcast.21, f32[128]{0:T(128)S(1)} %get-tuple-element.14, s32[128]{0:T(128)S(1)} %get-tuple-element.6), kind=kOutput, calls=%fused_computation.2 | convolution fusion | flops 403013632 | bytes 4195328 | tf_op jit(solution)/shard_map/dot_general | solution.py:274
  240.3 0.0 copy-done.2
  240.3 0.0 copy-start.7
  240.3 0.0 copy-start.8
  240.3 3.0 %fusion.47 = (f32[128]{0:T(128)S(1)}, f32[128,2048]{1,0:T(8,128)S(1)}) fusion(f32[128,2048]{1,0:T(8,128)S(1)} %copy-done.2, f32[128,2048]{1,0:T(8,128)S(1)} %convolution_multiply_fusion, f32[128,2048]{1,0:T(8,128)S(1)} %convolution_multiply_fusion.1, f32[128,2048]{1,0:T(8,128)S(1)} %convolution_multiply_fusion.2, bf16[768,2048]{1,0:T(8,128)(2,1)} %bitcast.21, ...), kind=kOutput, calls=%fused_computation.98 | convolution fusion | flops 405110656 | bytes 8914432 | tf_op jit(solution)/shard_map/dot_general | solution.py:274
  243.3 0.3 multiply_reduce_fusion
  243.6 0.0 copy-done.7
  243.6 0.0 copy-done.8
  243.6 1.0 fusion.20
  (24 shorter events, 0.3 us)
Async XLA Ops:
  0.0 149.3 %copy-start = (bf16[1,512,2048]{2,1,0:T(8,128)(2,1)S(1)}, bf16[1,512,2048]{2,1,0:T(8,128)(2,1)}, u32[]{:S(2)}) copy-start(bf16[1,512,2048]{2,1,0:T(8,128)(2,1)} %param.34) | copy-start | bytes 6291460
  41.7 16.9 %copy-start.4 = (bf16[1,128,2048]{2,1,0:T(8,128)(2,1)S(1)}, bf16[1,128,2048]{2,1,0:T(8,128)(2,1)}, u32[]{:S(2)}) copy-start(bf16[1,128,2048]{2,1,0:T(8,128)(2,1)} %param.20) | copy-start | bytes 1572868
  41.7 16.9 %copy-start.10 = (f32[1024]{0:T(1024)S(1)}, f32[1024]{0:T(1024)}, u32[]{:S(2)}) copy-start(f32[1024]{0:T(1024)} %param.26) | copy-start | bytes 12292
  58.6 6.5 %copy-start.5 = (f32[2048]{0:T(1024)S(1)}, f32[2048]{0:T(1024)}, u32[]{:S(2)}) copy-start(f32[2048]{0:T(1024)} %param.29) | copy-start | bytes 24580
  58.6 6.5 %copy-start.6 = (f32[2048]{0:T(1024)S(1)}, f32[2048]{0:T(1024)}, u32[]{:S(2)}) copy-start(f32[2048]{0:T(1024)} %param.28) | copy-start | bytes 24580
  61.8 1.0 copy-start.1
  67.5 78.8 %copy-start.11 = (bf16[1,2048,512]{2,1,0:T(8,128)(2,1)S(1)}, bf16[1,2048,512]{2,1,0:T(8,128)(2,1)}, u32[]{:S(2)}) copy-start(bf16[1,2048,512]{2,1,0:T(8,128)(2,1)} %param.32) | copy-start | bytes 6291460
  144.7 1.7 copy-start.3
  157.4 4.1 %copy-start.9 = (f32[1,128,4]{1,2,0:T(4,128)S(1)}, f32[1,128,4]{1,2,0:T(4,128)}, u32[]{:S(2)}) copy-start(f32[1,128,4]{1,2,0:T(4,128)} %param.31) | copy-start | bytes 6148
  157.4 75.2 %all-to-all-start.1 = ((bf16[32,24,2048]{2,1,0:T(8,128)(2,1)}), bf16[32,24,2048]{2,1,0:T(8,128)(2,1)}, u32[]{:S(2)}, u32[]{:S(2)}) async-start(bf16[32,24,2048]{2,1,0:T(8,128)(2,1)} %bitcast.86), calls=%async_computation.1 | async-start | bytes 6291456 | tf_op jit(solution)/shard_map/all_to_all | solution.py:267
  237.7 2.6 %copy-start.2 = (f32[128,2048]{1,0:T(8,128)S(1)}, f32[128,2048]{1,0:T(8,128)}, u32[]{:S(2)}) copy-start(f32[128,2048]{1,0:T(8,128)} %fusion.14) | copy-start | bytes 3145732
  240.3 3.3 %copy-start.7 = (f32[2048]{0:T(1024)S(1)}, f32[2048]{0:T(1024)}, u32[]{:S(2)}) copy-start(f32[2048]{0:T(1024)} %param.39) | copy-start | bytes 24580
  240.3 3.3 %copy-start.8 = (f32[2048]{0:T(1024)S(1)}, f32[2048]{0:T(1024)}, u32[]{:S(2)}) copy-start(f32[2048]{0:T(1024)} %param.38) | copy-start | bytes 24580

commit v2 on v1

--- a/solution.py
+++ b/solution.py
@@ -182,6 +182,144 @@
         ],
         out_specs=pl.BlockSpec((rows, PAIR * VALUE_HEAD_WIDTH), lambda step: (0, step)),
     )(offset, query_full.reshape(steps, PAIR, rows, width), whole, up_weight)
+
+
+def dispatch_kernel(
+    first_ref, pick_ref, out_ref, held, outgoing,
+    line_send, line_recv, send_sem, recv_sem, own_sem,
+):
+    count, ways = lax.axis_size("sp"), lax.axis_size("dp")
+    inner = inner_of(count)
+    outer = count // inner
+    plane = inner * ways
+    me = lax.axis_index("sp")
+    far, near = me // inner, me % inner
+    place = near * ways + lax.axis_index("dp")
+    up_ok, down_ok = far < outer - 1, far > 0
+    up = {"sp": jnp.minimum(far + 1, outer - 1) * inner + near}
+    down = {"sp": jnp.maximum(far - 1, 0) * inner + near}
+
+    def peer_of(step):
+        peer = (place + step) % plane
+        return peer, {"sp": far * inner + peer // ways, "dp": peer % ways}
+
+    barrier = pltpu.get_barrier_semaphore()
+
+    def greet(target):
+        pl.semaphore_signal(barrier, inc=1, device_id=target, device_id_type=MESH)
+
+    for step in range(1, outer):
+        greet({"sp": ((far + step) % outer) * inner + near})
+
+    @pl.loop(1, plane)
+    def _(step):
+        greet(peer_of(step)[1])
+
+    pl.semaphore_wait(barrier, outer + plane - 2)
+
+    def along(source, owner, side):
+        return pltpu.make_async_remote_copy(
+            src_ref=source,
+            dst_ref=held.at[owner],
+            send_sem=line_send.at[side, owner],
+            recv_sem=line_recv.at[owner],
+            device_id=(up, down)[side],
+            device_id_type=MESH,
+        )
+
+    def across(owner, step):
+        peer, target = peer_of(step)
+        return pltpu.make_async_remote_copy(
+            src_ref=outgoing.at[owner, peer],
+            dst_ref=out_ref.at[owner, place],
+            send_sem=send_sem.at[owner, peer],
+            recv_sem=recv_sem.at[owner, place],
+            device_id=target,
+            device_id_type=MESH,
+        )
+
+    def own_copy(owner):
+        return pltpu.make_async_copy(
+            outgoing.at[owner, place], out_ref.at[owner, place], own_sem.at[owner]
+        )
+
+    def spread(block, owner):
+        rows = jnp.dot(pick_ref[owner], block, preferred_element_type=jnp.float32)
+        outgoing[owner] = rows.reshape(outgoing.shape[1:]).astype(outgoing.dtype)
+
+        @pl.loop(1, plane)
+        def _(step):
+            across(owner, step).start()
+
+        own_copy(owner).start()
+
+    pl.when(up_ok)(lambda: along(first_ref, far, 0).start())
+    pl.when(down_ok)(lambda: along(first_ref, far, 1).start())
+    spread(first_ref[...], far)
+    for step in range(1, outer):
+        @pl.when(far >= step)
+        def _():
+            owner = far - step
+            along(first_ref, owner, 0).wait_recv()
+            pl.when(up_ok)(lambda: along(held.at[owner], owner, 0).start())
+            spread(held[owner], owner)
+
+        @pl.when(far + step < outer)
+        def _():
+            owner = far + step
+            along(first_ref, owner, 1).wait_recv()
+            pl.when(down_ok)(lambda: along(held.at[owner], owner, 1).start())
+            spread(held[owner], owner)
+
+    for owner in range(outer):
+        @pl.when(up_ok & (far >= owner))
+        def _():
+            along(first_ref, owner, 0).wait_send()
+
+        @pl.when(down_ok & (far <= owner))
+        def _():
+            along(first_ref, owner, 1).wait_send()
+
+        own_copy(owner).wait()
+
+        @pl.loop(1, plane)
+        def _(step):
+            across(owner, step).wait_send()
+            peer, target = peer_of(step)
+            pltpu.make_async_remote_copy(
+                src_ref=outgoing.at[owner, peer],
+                dst_ref=out_ref.at[owner, peer],
+                send_sem=send_sem.at[owner, peer],
+                recv_sem=recv_sem.at[owner, peer],
+                device_id=target,
+                device_id_type=MESH,
+            ).wait_recv()
+
+
+def dispatch_rows(first, picks, slots):
+    count, ways = lax.axis_size("sp"), lax.axis_size("dp")
+    inner = inner_of(count)
+    outer = count // inner
+    plane = inner * ways
+    shape = (outer, plane, slots, first.shape[1])
+    return pl.pallas_call(
+        dispatch_kernel,
+        out_shape=jax.ShapeDtypeStruct(shape, first.dtype),
+        in_specs=[pl.BlockSpec(memory_space=pltpu.VMEM)] * 2,
+        out_specs=pl.BlockSpec(memory_space=pltpu.VMEM),
+        scratch_shapes=[
+            pltpu.VMEM((outer,) + first.shape, first.dtype),
+            pltpu.VMEM(shape, first.dtype),
+            pltpu.SemaphoreType.DMA((2, outer)),
+            pltpu.SemaphoreType.DMA((outer,)),
+            pltpu.SemaphoreType.DMA((outer, plane)),
+            pltpu.SemaphoreType.DMA((outer, plane)),
+            pltpu.SemaphoreType.DMA((outer,)),
+        ],
+        compiler_params=pltpu.CompilerParams(
+            collective_id=1, has_side_effects=True, vmem_limit_bytes=40 * 2**20
+        ),
+    )(first, picks)
 
 
 def swiglu_rows(rows, gate_mat, up_mat, down_mat):
@@ -219,8 +357,24 @@
     local_pos = start + jnp.arange(tok_rows, dtype=jnp.int32)
     cos_local, sin_local = rotation_tables(local_pos, QK_ROPE)
     keys_turned = turn(keys_rope[0].astype(jnp.float32), cos_local, sin_local).astype(jnp.bfloat16)
+    group = lax.axis_size("sp") * lax.axis_size("dp")
+    capacity = (tok_rows * TOP_K * 3 + 2 * group - 1) // (2 * group)
+    entries = expert_ids[0].reshape(-1)
+    onehot = (entries[:, None] == jnp.arange(group, dtype=jnp.int32)[None, :]).astype(jnp.int32)
+    earlier = jnp.cumsum(onehot, axis=0) - onehot
+    slots = jnp.sum(earlier * onehot, axis=-1)
+    places = (entries * capacity + slots).reshape(tok_rows, TOP_K)
+    tags = jnp.concatenate([expert_ids[0], slots.reshape(tok_rows, TOP_K)], axis=1)
     whole = gather_rows(
-        jnp.concatenate([normed, jnp.pad(keys_turned, ((0, 0), (0, LANES - QK_ROPE)))], axis=1)
+        jnp.concatenate(
+            [
+                normed,
+                keys_turned,
+                tags.astype(jnp.bfloat16),
+                jnp.zeros((tok_rows, LANES - QK_ROPE - 2 * TOP_K), jnp.bfloat16),
+            ],
+            axis=1,
+        )
     )
     query_heads = queries[0].reshape(tok_rows, ATTENTION_HEADS, PLAIN_HEAD_WIDTH + QK_ROPE)
     query_turned = turn(
@@ -245,19 +399,22 @@
     first = layer_norm(
         ALPHA * hidden_in[0].astype(jnp.float32) + mixed, norm1_gain, norm1_bias
     ).astype(jnp.bfloat16)
-    group = lax.axis_size("sp") * lax.axis_size("dp")
-    capacity = (tok_rows * TOP_K * 3 + 2 * group - 1) // (2 * group)
-    entries = expert_ids[0].reshape(-1)
-    onehot = (entries[:, None] == jnp.arange(group, dtype=jnp.int32)[None, :]).astype(jnp.int32)
-    earlier = jnp.cumsum(onehot, axis=0) - onehot
-    slots = jnp.sum(earlier * onehot, axis=-1)
-    places = (entries * capacity + slots).reshape(tok_rows, TOP_K)
     slot_ids = jnp.arange(group * capacity, dtype=jnp.int32)
-    dispatch = jnp.any(places[None, :, :] == slot_ids[:, None, None], axis=-1).astype(jnp.bfloat16)
-    outbound = jnp.dot(dispatch, first, preferred_element_type=jnp.float32).astype(jnp.bfloat16)
-    arrived = lax.all_to_all(
-        outbound.reshape(group, capacity, D), ("sp", "dp"), split_axis=0, concat_axis=0, tiled=True
-    )
+    inner = inner_of(lax.axis_size("sp"))
+    plane = inner * lax.axis_size("dp")
+    room = -(-capacity // 8) * 8
+    far, near = lax.axis_index("sp") // inner, lax.axis_index("sp") % inner
+    tag_from = key_value_latent.shape[2] + QK_ROPE
+    line_tags = lax.dynamic_index_in_dim(
+        whole[:, tag_from : tag_from + 2 * TOP_K].reshape(-1, inner, tok_rows, 2 * TOP_K),
+        near, axis=1, keepdims=False,
+    ).astype(jnp.int32)
+    line_rows = (line_tags[..., :TOP_K] - far * plane) * room + line_tags[..., TOP_K:]
+    row_ids = jnp.arange(plane * room, dtype=jnp.int32)
+    picks = jnp.any(
+        line_rows[:, None, :, :] == row_ids[None, :, None, None], axis=-1
+    ).astype(jnp.bfloat16)
+    arrived = dispatch_rows(first, picks, room)[:, :, :capacity]
     flat_rows = arrived.reshape(group * capacity, D)
     produced = (
         swiglu_rows(flat_rows, gate_proj[0], up_proj[0], down_proj[0])

time: 245 us -> 221 us (0.902)
  blocking collectives: 77.1 us -> 0 us
  Pallas kernels: 43.9 us -> 94.8 us
  local copies, waits for them, and re-layouts: 13.4 us -> 16.7 us
    all_to_all x1 -> x0, blocking collectives: 77.1 us -> none  [per_device(): lax.all_to_all(outbound.reshape(group, capacity, D), ('sp', 'dp'), split_...]
    pallas_call x0 -> x1, Pallas kernels: none -> 50.9 us  [dispatch_rows(): pl.pallas_call(dispatch_kernel, out_shape=jax.ShapeDtypeStruct(shape, fir...]
    unnamed x26 -> x30, local copies, waits for them, and re-layouts: 4.88 us -> 5.77 us
where the time goes in v2:
time: 221 us
  Pallas kernels  94.8 us (43%)
  waiting for transfers between devices  64.6 us (29%)
  matrix products  30.9 us (14%)
  local copies, waits for them, and re-layouts  16.7 us (8%)
  other arithmetic  9.47 us (4%)
  starting transfers between devices  3.84 us (2%)
    all_to_all x1, waiting for transfers between devices, per_device(): lax.all_to_all(produced, ('sp', 'dp'), split_axis=0, concat_axis=0, tiled...  64.6 us
    pallas_call x1, Pallas kernels, dispatch_rows(): pl.pallas_call(dispatch_kernel, out_shape=jax.ShapeDtypeStruct(shape, fir...  50.9 us
    pallas_call x1, Pallas kernels, gather_rows(): pl.pallas_call(functools.partial(gather_kernel, count), out_shape=jax.Sha...  28.1 us
    pallas_call x1, Pallas kernels, attend(): pl.pallas_call(attend_kernel, grid=(steps,), out_shape=jax.ShapeDtypeStru...  15.8 us
    dot_general x2, matrix products, swiglu_rows(): return jnp.dot(inner, down_mat, preferred_element_type=jnp.float32)  12.2 us
    dot_general x4, matrix products, per_device(): picked = jnp.dot(picker, returned_flat, preferred_element_type=jnp.float32)  10.6 us
    unnamed x30, local copies, waits for them, and re-layouts  5.77 us
    dot_general x2, matrix products, swiglu_rows(): gated = jnp.dot(rows, gate_mat, preferred_element_type=jnp.float32)  4.96 us
  transfers between devices with their start and end apart: 1, of which 1 were waited for; matrix products, arithmetic and copies ran while one was open for 3% of the time, Pallas kernels for 0%

profile of v2, /device:TPU:0, one launch (start us, length us, event | category | flops | bytes accessed | tf_op | source)
XLA Modules:
  0.0 220.7 jit_solution(5435455135515746538)
XLA Ops:
  0.0 0.0 copy-start
  0.0 1.4 copy.51
  1.4 0.0 copy-start.11
  1.5 0.8 copy.59
  2.2 0.1 eq.104
  2.4 0.1 eq.100
  2.5 0.6 convert_bitcast_fusion
  3.1 0.8 copy.58
  3.9 0.9 add_convert_fusion.3
  4.9 0.1 copy.54
  5.0 0.1 add_convert_fusion.2
  5.0 0.3 copy.56
  5.3 0.3 copy.57
  5.6 1.0 copy.55
  6.6 1.2 reduce-window.6
  7.8 0.2 slice_reduce_fusion.4
  8.1 0.1 fusion.39
  8.2 0.1 reshape.166
  8.3 1.0 fusion.21
  9.3 0.0 copy-done.11
  9.3 1.0 fusion.23
  10.4 1.6 concatenate.15.x_ref
  11.9 28.1 %shard_map.190 = bf16[8,128,640]{2,1,0:T(8,128)(2,1)} custom-call(bf16[128,640]{1,0:T(8,128)(2,1)} %concatenate.15.x_ref), custom_call_target="tpu_custom_call" | custom-call | tf_op jit(solution)/shard_map/pallas_call | solution.py:124
  40.0 1.1 slice.84
  41.1 0.9 broadcast_in_dim.6
  42.1 0.9 broadcast_in_dim.7
  43.0 4.0 %concatenate.14 = bf16[128,16,256]{2,0,1:T(8,128)(2,1)} concatenate(bf16[128,16,64]{2,0,1:T(8,128)(2,1)} %copy.55, bf16[128,16,64]{2,0,1:T(8,128)(2,1)} %broadcast_in_dim.6, bf16[128,16,16]{2,0,1:T(8,128)(2,1)S(1)} %copy.56, bf16[128,16,16]{2,0,1:T(8,128)(2,1)S(1)} %copy.57, bf16[128,16,96]{2,0,1:T(8,128)(2,1)} %broadcast_in_dim.7), dimensions={2} | concatenate | bytes 2097152 | tf_op jit(solution)/shard_map/concatenate | solution.py:385
  46.9 15.8 %shard_map.191 = bf16[128,1024]{1,0:T(8,128)(2,1)} custom-call(s32[1]{0:T(128)} %bitcast.1.offset_ref, bf16[8,2,128,256]{3,2,1,0:T(8,128)(2,1)} %bitcast.88, bf16[1024,640]{1,0:T(8,128)(2,1)} %bitcast.87, bf16[512,2048]{1,0:T(8,128)(2,1)} %up_ref.1), custom_call_target="tpu_custom_call" | custom-call | tf_op jit(solution)/shard_map/pallas_call | solution.py:173
  62.8 1.1 fusion.17
  63.8 0.0 copy-done.4
  63.9 0.0 copy-done.10
  63.9 0.0 copy-start.5
  63.9 0.0 copy-start.6
  63.9 3.2 %fusion.45 = (f32[128]{0:T(128)S(1)}, f32[128,2048]{1,0:T(8,128)S(1)}) fusion(bf16[1024,2048]{1,0:T(8,128)(2,1)} %param.27, bf16[128,1024]{1,0:T(8,128)(2,1)} %shard_map.191, f32[1024]{0:T(1024)S(1)} %copy-done.10, f32[128]{0:T(128)S(1)} %add_rsqrt_fusion.2, bf16[1,128,2048]{2,1,0:T(8,128)(2,1)S(1)} %copy-done.4), kind=kOutput, calls=%fused_computation.97 | convolution fusion | flops 538443648 | bytes 6034432 | tf_op jit(solution)/shard_map/dot_general | solution.py:398
  67.1 0.0 copy-start.2
  67.1 1.0 copy-done.2
  68.1 0.3 multiply_reduce_fusion.1
  68.3 0.1 copy.65
  68.5 0.2 fusion.10
  68.8 0.0 copy-done.5
  68.8 0.0 copy-done.6
  68.8 1.5 add_convert_fusion.1.first_ref
  70.2 0.0 copy-start.12
  70.3 50.9 %shard_map.192 = bf16[4,8,24,2048]{3,2,1,0:T(8,128)(2,1)S(1)} custom-call(bf16[128,2048]{1,0:T(8,128)(2,1)S(1)} %add_convert_fusion.1.first_ref, bf16[4,192,128]{2,1,0:T(8,128)(2,1)S(1)} %convert_element_type.92.pick_ref), custom_call_target="tpu_custom_call" | custom-call | tf_op jit(solution)/shard_map/pallas_call | solution.py:305
  121.1 0.0 copy-start.1
  121.2 1.7 copy-done.1
  122.8 0.0 copy-done.12
  122.9 2.9 %fusion.8 = f32[768,512]{1,0:T(8,128)} fusion(bf16[768,2048]{1,0:T(8,128)(2,1)S(1)} %bitcast.84, bf16[1,2048,512]{2,1,0:T(8,128)(2,1)S(1)} %copy-done.12), kind=kOutput, calls=%fused_computation.14 | convolution fusion | flops 1610612736 | bytes 6815744 | tf_op jit(solution)/shard_map/dot_general | solution.py:326
  125.8 0.0 copy-done
  125.8 8.1 %convolution_convert_fusion = bf16[768,2048]{1,0:T(8,128)(2,1)} fusion(bf16[1,512,2048]{2,1,0:T(8,128)(2,1)S(1)} %copy-done, f32[768,512]{1,0:T(8,128)} %fusion.8, bf16[768,2048]{1,0:T(8,128)(2,1)} %bitcast.85, bf16[1,2048,512]{2,1,0:T(8,128)(2,1)} %param.33), kind=kOutput, calls=%fused_computation | convolution fusion | flops 3225157632 | bytes 12058624 | tf_op jit(solution)/shard_map/dot_general | solution.py:329
  133.9 3.8 %all-to-all-start = ((bf16[32,24,2048]{2,1,0:T(8,128)(2,1)}), bf16[32,24,2048]{2,1,0:T(8,128)(2,1)}, u32[]{:S(2)}, u32[]{:S(2)}) async-start(bf16[32,24,2048]{2,1,0:T(8,128)(2,1)} %bitcast.89), calls=%async_computation | async-start | bytes 6291456 | tf_op jit(solution)/shard_map/all_to_all | solution.py:424
  137.8 0.2 slice_reduce_fusion.3
  138.1 2.0 fusion.47
  140.1 4.1 %fusion.14 = f32[128,2048]{1,0:T(8,128)} fusion(bf16[512,2048]{1,0:T(8,128)(2,1)} %param.37, bf16[128,2048]{1,0:T(8,128)(2,1)S(1)} %add_convert_fusion.1.first_ref, bf16[2048,512]{1,0:T(8,128)(2,1)} %param.36, f32[128,512]{1,0:T(8,128)S(1)} %fusion.47), kind=kOutput, calls=%fused_computation.21 | convolution fusion | flops 537264128 | bytes 6029312 | tf_op jit(solution)/shard_map/dot_general | solution.py:329
  144.2 64.6 %all-to-all-done = bf16[32,24,2048]{2,1,0:T(8,128)(2,1)} async-done(((bf16[32,24,2048]{2,1,0:T(8,128)(2,1)}), bf16[32,24,2048]{2,1,0:T(8,128)(2,1)}, u32[]{:S(2)}, u32[]{:S(2)}) %all-to-all-start) | async-done | bytes 3145760 | tf_op jit(solution)/shard_map/all_to_all | solution.py:424
  208.8 2.5 %convolution_multiply_fusion.1 = f32[128,2048]{1,0:T(8,128)S(1)} fusion(bf16[768,2048]{1,0:T(8,128)(2,1)} %bitcast.23, f32[128]{0:T(128)S(1)} %get-tuple-element.17, s32[128]{0:T(128)S(1)} %get-tuple-element.7), kind=kOutput, calls=%fused_computation.2 | convolution fusion | flops 403013632 | bytes 4195328 | tf_op jit(solution)/shard_map/dot_general | solution.py:431
  211.3 2.5 %convolution_multiply_fusion.2 = f32[128,2048]{1,0:T(8,128)S(1)} fusion(bf16[768,2048]{1,0:T(8,128)(2,1)} %bitcast.23, f32[128]{0:T(128)S(1)} %get-tuple-element.18, s32[128]{0:T(128)S(1)} %get-tuple-element.8), kind=kOutput, calls=%fused_computation.3 | convolution fusion | flops 403013632 | bytes 4195328 | tf_op jit(solution)/shard_map/dot_general | solution.py:431
  213.8 0.0 copy-start.3
  213.8 2.6 %convolution_multiply_fusion = f32[128,2048]{1,0:T(8,128)S(1)} fusion(bf16[768,2048]{1,0:T(8,128)(2,1)} %bitcast.23, f32[128]{0:T(128)S(1)} %get-tuple-element.16, s32[128]{0:T(128)S(1)} %get-tuple-element.6), kind=kOutput, calls=%fused_computation.1 | convolution fusion | flops 403013632 | bytes 4195328 | tf_op jit(solution)/shard_map/dot_general | solution.py:431
  216.4 0.0 copy-start.7
  216.4 0.0 copy-start.8
  216.4 3.0 %fusion.46 = (f32[128]{0:T(128)S(1)}, f32[128,2048]{1,0:T(8,128)S(1)}) fusion(f32[128,2048]{1,0:T(8,128)S(1)} %copy-done.3, f32[128,2048]{1,0:T(8,128)S(1)} %convolution_multiply_fusion, f32[128,2048]{1,0:T(8,128)S(1)} %convolution_multiply_fusion.1, f32[128,2048]{1,0:T(8,128)S(1)} %convolution_multiply_fusion.2, bf16[768,2048]{1,0:T(8,128)(2,1)} %bitcast.23, ...), kind=kOutput, calls=%fused_computation.98 | convolution fusion | flops 405110656 | bytes 8914432 | tf_op jit(solution)/shard_map/dot_general | solution.py:431
  219.4 0.3 multiply_reduce_fusion
  219.7 1.0 fusion.20
  (31 shorter events, 0.3 us)
Async XLA Ops:
  0.0 125.8 %copy-start = (bf16[1,512,2048]{2,1,0:T(8,128)(2,1)S(1)}, bf16[1,512,2048]{2,1,0:T(8,128)(2,1)}, u32[]{:S(2)}) copy-start(bf16[1,512,2048]{2,1,0:T(8,128)(2,1)} %param.34) | copy-start | bytes 6291460
  1.4 7.9 %copy-start.11 = (f32[512]{0:T(512)S(1)}, f32[512]{0:T(512)}, u32[]{:S(2)}) copy-start(f32[512]{0:T(512)} %param.24) | copy-start | bytes 6148
  46.9 16.9 %copy-start.4 = (bf16[1,128,2048]{2,1,0:T(8,128)(2,1)S(1)}, bf16[1,128,2048]{2,1,0:T(8,128)(2,1)}, u32[]{:S(2)}) copy-start(bf16[1,128,2048]{2,1,0:T(8,128)(2,1)} %param.20) | copy-start | bytes 1572868
  46.9 16.9 %copy-start.10 = (f32[1024]{0:T(1024)S(1)}, f32[1024]{0:T(1024)}, u32[]{:S(2)}) copy-start(f32[1024]{0:T(1024)} %param.26) | copy-start | bytes 12292
  63.9 4.9 %copy-start.5 = (f32[2048]{0:T(1024)S(1)}, f32[2048]{0:T(1024)}, u32[]{:S(2)}) copy-start(f32[2048]{0:T(1024)} %param.29) | copy-start | bytes 24580
  63.9 4.9 %copy-start.6 = (f32[2048]{0:T(1024)S(1)}, f32[2048]{0:T(1024)}, u32[]{:S(2)}) copy-start(f32[2048]{0:T(1024)} %param.28) | copy-start | bytes 24580
  67.1 1.0 copy-start.2
  70.2 52.6 %copy-start.12 = (bf16[1,2048,512]{2,1,0:T(8,128)(2,1)S(1)}, bf16[1,2048,512]{2,1,0:T(8,128)(2,1)}, u32[]{:S(2)}) copy-start(bf16[1,2048,512]{2,1,0:T(8,128)(2,1)} %param.32) | copy-start | bytes 6291460
  121.1 1.7 copy-start.1
  133.9 3.9 %copy-start.9 = (f32[1,128,4]{1,2,0:T(4,128)S(1)}, f32[1,128,4]{1,2,0:T(4,128)}, u32[]{:S(2)}) copy-start(f32[1,128,4]{1,2,0:T(4,128)} %param.31) | copy-start | bytes 6148
  133.9 74.8 %all-to-all-start = ((bf16[32,24,2048]{2,1,0:T(8,128)(2,1)}), bf16[32,24,2048]{2,1,0:T(8,128)(2,1)}, u32[]{:S(2)}, u32[]{:S(2)}) async-start(bf16[32,24,2048]{2,1,0:T(8,128)(2,1)} %bitcast.89), calls=%async_computation | async-start | bytes 6291456 | tf_op jit(solution)/shard_map/all_to_all | solution.py:424
  213.8 2.6 %copy-start.3 = (f32[128,2048]{1,0:T(8,128)S(1)}, f32[128,2048]{1,0:T(8,128)}, u32[]{:S(2)}) copy-start(f32[128,2048]{1,0:T(8,128)} %fusion.14) | copy-start | bytes 3145732
  216.4 3.3 %copy-start.7 = (f32[2048]{0:T(1024)S(1)}, f32[2048]{0:T(1024)}, u32[]{:S(2)}) copy-start(f32[2048]{0:T(1024)} %param.39) | copy-start | bytes 24580
  216.4 3.3 %copy-start.8 = (f32[2048]{0:T(1024)S(1)}, f32[2048]{0:T(1024)}, u32[]{:S(2)}) copy-start(f32[2048]{0:T(1024)} %param.38) | copy-start | bytes 24580
